TPU v7x, 32 devices: a whole 2x2x4 slice. The times are simulated.
32 devices in a mesh: sp: 8 (over z, y), tp: 4 (over x, core).
Axes of the slice: x: 2, y: 2, z: 4, core: 2. Of those that a mesh axis runs over, the one named last changes fastest.
Arguments:
- activations: bfloat16 [2, 256, 1024], P(None, 'sp', 'tp'), may hold values from -6 to 6
- norm_gain: float32 [4, 1024], replicated, may hold values from 0.1 to 1.9
- in_weight: bfloat16 [4, 1024, 512], P(None, 'sp', 'tp'), may hold values from -0.1875 to 0.1875
- out_weight: bfloat16 [4, 512, 1024], P(None, 'tp', 'sp'), may hold values from -0.25 to 0.25
- mixing: bfloat16 [4, 4, 128, 128], P(None, 'tp', 'sp'), may hold values from -0.5 to 0.5
- pool_scale: float32 [4, 512], P(None, 'tp'), may hold values from 0.1 to 1.9
Outputs:
- result: bfloat16 [2, 256, 1024], P(None, 'sp', 'tp')
All inputs are finite; a program needn't handle non-finite values.
Results may differ from a plain program's by a relative error of at most 0.03.
Values may be sent and summed in bfloat16 or wider, within the bound.
A program may use at most 64 MiB of HBM per device.

v0:
```python
import jax
import jax.numpy as jnp
from jax import lax
from jax.sharding import PartitionSpec as P


def taken_in(x, axis, dim, absorb, carry):
    whole = jax.tree.map(lambda part: lax.all_gather(part, axis, axis=dim, tiled=True), x)
    return absorb(carry, whole, jnp.int32(0))


def for_sending(x):
    return jax.tree.map(lambda a: a.astype(jnp.bfloat16) if a.dtype == jnp.float32 else a, x)


def extended_2(cells, sides, width, closed):
    for axis, dim in sides:
        count = lax.axis_size(axis)
        ends = count if closed else count - 1
        head = lax.slice_in_dim(cells, 0, width, axis=dim)
        tail = lax.slice_in_dim(cells, cells.shape[dim] - width, cells.shape[dim], axis=dim)
        cells = jnp.concatenate(
            [
                lax.ppermute(tail, axis, [(i, (i + 1) % count) for i in range(ends)]),
                cells,
                lax.ppermute(head, axis, [((i + 1) % count, i) for i in range(ends)]),
            ],
            axis=dim,
        )
    return cells


def scattered(product, width, axis):
    everything = product(jnp.int32(0), lax.axis_size(axis) * width)
    own = lax.psum_scatter(everything.astype(jnp.bfloat16), axis, scatter_dimension=0, tiled=True)
    return own.astype(jnp.float32)


def fetch_output(out_weight, mixing, layer_index):
    return (
        lax.all_gather(out_weight[layer_index], "sp", axis=1, tiled=True),
        lax.all_gather(mixing[layer_index], "sp", axis=1, tiled=True),
    )


def fold_input(shard_rows, flat_rows):

    def add_rows(running, block_rows, first_row):
        left_cols = lax.dynamic_slice_in_dim(flat_rows, first_row, block_rows.shape[0], 1)
        return running + jnp.dot(left_cols, block_rows, preferred_element_type=jnp.float32)

    initial = jnp.zeros((flat_rows.shape[0], shard_rows.shape[1]), jnp.float32)
    return taken_in(for_sending(shard_rows), "sp", 0, add_rows, initial)


def run_layer(state_now, gain_row, project_in, output_block, mixing_block, scale_row):
    num_seqs, tok_count, _ = state_now.shape
    gathered = lax.all_gather(state_now, "tp", axis=2, tiled=True)
    model_width = gathered.shape[2]
    state_f32 = gathered.astype(jnp.float32)
    normed = (
        state_f32
        * lax.rsqrt(jnp.mean(state_f32 * state_f32, axis=-1, keepdims=True) + 1e-06)
        * gain_row
    ).astype(jnp.bfloat16)
    flat_rows = normed.reshape(num_seqs * tok_count, model_width)
    pooled_in = project_in(flat_rows).astype(jnp.bfloat16).reshape(num_seqs, tok_count, -1)
    extended = extended_2(pooled_in, (("sp", 1),), 8, False)
    seq_len = tok_count * lax.axis_size("sp")
    offset = lax.axis_index("sp") * tok_count
    positions = offset + jnp.arange(tok_count, dtype=jnp.int32)
    ext_positions = offset + jnp.arange(tok_count + 16, dtype=jnp.int32) - 8
    local_groups = mixing_block.shape[0]
    group_width = mixing_block.shape[1]
    outputs = []
    for group_slot in range(local_groups):
        group_number = lax.axis_index("tp") * local_groups + group_slot
        window = jnp.left_shift(jnp.int32(2), group_number)
        window_low = positions - window // 2
        window_high = window_low + window
        inside = (ext_positions[None, :] >= window_low[:, None]) & (
            ext_positions[None, :] < window_high[:, None]
        )
        band_rows = inside.astype(jnp.bfloat16)
        counts = (jnp.clip(window_high, 0, seq_len) - jnp.clip(window_low, 0, seq_len)).astype(
            jnp.float32
        )
        columns = slice(group_slot * group_width, (group_slot + 1) * group_width)
        part_sums = jnp.einsum(
            "tj,bjc->btc", band_rows, extended[..., columns], preferred_element_type=jnp.float32
        )
        window_mean = part_sums / counts[None, :, None]
        centred = (window_mean - pooled_in[..., columns].astype(jnp.float32)).astype(jnp.bfloat16)
        mixed_group = jnp.einsum(
            "btc,cd->btd", centred, mixing_block[group_slot], preferred_element_type=jnp.float32
        )
        outputs.append(mixed_group * scale_row[columns])
    joined = (
        jnp.concatenate(outputs, axis=-1).astype(jnp.bfloat16).reshape(num_seqs * tok_count, -1)
    )

    def term_rows(first_row, row_count):
        weight_cols = lax.dynamic_slice_in_dim(output_block, first_row, row_count, 1)
        return lax.dot_general(
            weight_cols, joined, (((0,), (1,)), ((), ())), preferred_element_type=jnp.float32
        )

    own_rows = output_block.shape[1] // lax.axis_size("tp")
    summed = scattered(term_rows, own_rows, "tp")
    return jnp.transpose(summed).reshape(num_seqs, tok_count, own_rows).astype(jnp.bfloat16)


def body(activations, norm_gain, in_weight, out_weight, mixing, pool_scale):
    layer_count = in_weight.shape[0]
    state_now = activations
    for layer_index in range(layer_count):
        output_block, mixing_block = fetch_output(out_weight, mixing, layer_index)

        def project_in(flat_rows, shard_rows=in_weight[layer_index]):
            return fold_input(shard_rows, flat_rows)

        state_now = run_layer(
            state_now,
            norm_gain[layer_index],
            project_in,
            output_block,
            mixing_block,
            pool_scale[layer_index],
        )
    return state_now


def solution(mesh):
    return jax.shard_map(
        body,
        mesh=mesh,
        in_specs=(
            P(None, "sp", "tp"),
            P(),
            P(None, "sp", "tp"),
            P(None, "tp", "sp"),
            P(None, "tp", "sp", None),
            P(None, "tp"),
        ),
        out_specs=P(None, "sp", "tp"),
        check_vma=False,
    )
```

profile of v0, /device:TPU:0, one launch (start us, length us, event | category | flops | bytes accessed | tf_op | source)
XLA Modules:
  0.0 458.6 jit_solution(8462057962873662359)
XLA Ops:
  6.5 0.9 fusion.111
  7.4 6.7 %all_gather.48 = bf16[2,32,1024]{2,1,0:T(8,128)(2,1)S(1)} all-gather(bf16[2,32,256]{2,1,0:T(8,128)(2,1)S(1)} %copy-done.2), channel_id=1, replica_groups=mesh['sp'=8,'tp'=4] {'tp'}, dimensions={2}, use_global_device_ids=true | all-gather | bytes 163840 | tf_op jit(solution)/shard_map/all_gather | solution.py:58
  14.1 0.1 fusion.20
  14.3 31.6 %all-gather = bf16[1,1024,128]{2,1,0:T(8,128)(2,1)S(1)} all-gather(bf16[1,128,128]{2,1,0:T(8,128)(2,1)S(1)} %get-tuple-element.13), channel_id=2, replica_groups=mesh['sp'=8,'tp'=4] {'sp'}, dimensions={1}, use_global_device_ids=true | all-gather | bytes 294912 | tf_op jit(solution)/shard_map/all_gather | solution.py:8
  45.9 0.1 fusion.22
  46.0 0.2 convolution_convert_fusion.7
  46.2 3.3 collective-permute-start
  49.5 1.3 collective-permute-start.1
  50.9 0.6 copy-done.3
  51.5 0.7 copy-done.4
  52.2 31.6 %all-gather.2 = bf16[1,128,1024]{2,1,0:T(8,128)(2,1)S(1)} all-gather(bf16[1,128,128]{2,1,0:T(8,128)(2,1)S(1)} %get-tuple-element.9), channel_id=4, replica_groups=mesh['sp'=8,'tp'=4] {'sp'}, dimensions={2}, use_global_device_ids=true | all-gather | bytes 294912 | tf_op jit(solution)/shard_map/all_gather | solution.py:41
  83.9 30.4 %all-gather.1 = bf16[1,1,128,128]{3,2,1,0:T(8,128)(2,1)S(1)} all-gather(bf16[1,1,16,128]{3,2,1,0:T(8,128)(2,1)S(1)} %get-tuple-element.27), channel_id=3, replica_groups=mesh['sp'=8,'tp'=4] {'sp'}, dimensions={2}, use_global_device_ids=true | all-gather | bytes 36864 | tf_op jit(solution)/shard_map/all_gather | solution.py:42
  114.3 0.3 fusion.13
  114.6 0.8 fusion
  115.5 30.9 %all-gather.3 = bf16[1,1024,128]{2,1,0:T(8,128)(2,1)S(1)} all-gather(bf16[1,128,128]{2,1,0:T(8,128)(2,1)S(1)} %get-tuple-element.12), channel_id=5, replica_groups=mesh['sp'=8,'tp'=4] {'sp'}, dimensions={1}, use_global_device_ids=true | all-gather | bytes 294912 | tf_op jit(solution)/shard_map/all_gather | solution.py:8
  146.4 30.9 %all-gather.5 = bf16[1,128,1024]{2,1,0:T(8,128)(2,1)S(1)} all-gather(bf16[1,128,128]{2,1,0:T(8,128)(2,1)S(1)} %get-tuple-element.8), channel_id=7, replica_groups=mesh['sp'=8,'tp'=4] {'sp'}, dimensions={2}, use_global_device_ids=true | all-gather | bytes 294912 | tf_op jit(solution)/shard_map/all_gather | solution.py:41
  177.4 5.6 %all_gather.52 = bf16[2,32,1024]{2,1,0:T(8,128)(2,1)S(1)} all-gather(bf16[2,32,256]{2,1,0:T(8,128)(2,1)} %bitcast.154), channel_id=1, replica_groups=mesh['sp'=8,'tp'=4] {'tp'}, dimensions={2}, use_global_device_ids=true | all-gather | bytes 163840 | tf_op jit(solution)/shard_map/all_gather | solution.py:58
  183.0 0.1 fusion.23
  183.1 0.1 fusion.25
  183.2 0.2 convolution_convert_fusion.6
  183.4 3.6 collective-permute-start.2
  187.0 1.3 collective-permute-start.3
  188.3 31.0 %all-gather.4 = bf16[1,1,128,128]{3,2,1,0:T(8,128)(2,1)S(1)} all-gather(bf16[1,1,16,128]{3,2,1,0:T(8,128)(2,1)S(1)} %get-tuple-element.28), channel_id=6, replica_groups=mesh['sp'=8,'tp'=4] {'sp'}, dimensions={2}, use_global_device_ids=true | all-gather | bytes 36864 | tf_op jit(solution)/shard_map/all_gather | solution.py:42
  219.3 0.3 fusion.15
  219.6 0.8 fusion.1
  220.5 30.7 %all-gather.6 = bf16[1,1024,128]{2,1,0:T(8,128)(2,1)S(1)} all-gather(bf16[1,128,128]{2,1,0:T(8,128)(2,1)S(1)} %get-tuple-element.14), channel_id=8, replica_groups=mesh['sp'=8,'tp'=4] {'sp'}, dimensions={1}, use_global_device_ids=true | all-gather | bytes 294912 | tf_op jit(solution)/shard_map/all_gather | solution.py:8
  251.3 31.0 %all-gather.8 = bf16[1,128,1024]{2,1,0:T(8,128)(2,1)S(1)} all-gather(bf16[1,128,128]{2,1,0:T(8,128)(2,1)S(1)} %get-tuple-element.10), channel_id=10, replica_groups=mesh['sp'=8,'tp'=4] {'sp'}, dimensions={2}, use_global_device_ids=true | all-gather | bytes 294912 | tf_op jit(solution)/shard_map/all_gather | solution.py:41
  282.3 5.6 %all_gather.56 = bf16[2,32,1024]{2,1,0:T(8,128)(2,1)S(1)} all-gather(bf16[2,32,256]{2,1,0:T(8,128)(2,1)} %bitcast.155), channel_id=1, replica_groups=mesh['sp'=8,'tp'=4] {'tp'}, dimensions={2}, use_global_device_ids=true | all-gather | bytes 163840 | tf_op jit(solution)/shard_map/all_gather | solution.py:58
  287.9 0.1 fusion.26
  288.0 0.1 fusion.28
  288.1 0.2 convolution_convert_fusion.5
  288.3 3.9 collective-permute-start.4
  292.2 1.3 collective-permute-start.5
  293.5 31.0 %all-gather.7 = bf16[1,1,128,128]{3,2,1,0:T(8,128)(2,1)S(1)} all-gather(bf16[1,1,16,128]{3,2,1,0:T(8,128)(2,1)S(1)} %get-tuple-element.30), channel_id=9, replica_groups=mesh['sp'=8,'tp'=4] {'sp'}, dimensions={2}, use_global_device_ids=true | all-gather | bytes 36864 | tf_op jit(solution)/shard_map/all_gather | solution.py:42
  324.5 0.3 fusion.17
  324.9 0.8 fusion.2
  325.7 30.7 %all-gather.9 = bf16[1,1024,128]{2,1,0:T(8,128)(2,1)S(1)} all-gather(bf16[1,128,128]{2,1,0:T(8,128)(2,1)S(1)} %get-tuple-element.11), channel_id=11, replica_groups=mesh['sp'=8,'tp'=4] {'sp'}, dimensions={1}, use_global_device_ids=true | all-gather | bytes 294912 | tf_op jit(solution)/shard_map/all_gather | solution.py:8
  356.5 31.0 %all-gather.11 = bf16[1,128,1024]{2,1,0:T(8,128)(2,1)S(1)} all-gather(bf16[1,128,128]{2,1,0:T(8,128)(2,1)S(1)} %get-tuple-element.7), channel_id=13, replica_groups=mesh['sp'=8,'tp'=4] {'sp'}, dimensions={2}, use_global_device_ids=true | all-gather | bytes 294912 | tf_op jit(solution)/shard_map/all_gather | solution.py:41
  387.5 5.6 %all_gather.60 = bf16[2,32,1024]{2,1,0:T(8,128)(2,1)S(1)} all-gather(bf16[2,32,256]{2,1,0:T(8,128)(2,1)} %bitcast.153), channel_id=1, replica_groups=mesh['sp'=8,'tp'=4] {'tp'}, dimensions={2}, use_global_device_ids=true | all-gather | bytes 163840 | tf_op jit(solution)/shard_map/all_gather | solution.py:58
  393.1 0.1 fusion.29
  393.2 0.1 fusion.31
  393.3 0.2 convolution_convert_fusion.4
  393.5 3.9 collective-permute-start.6
  397.4 1.3 collective-permute-start.7
  398.7 31.0 %all-gather.10 = bf16[1,1,128,128]{3,2,1,0:T(8,128)(2,1)S(1)} all-gather(bf16[1,1,16,128]{3,2,1,0:T(8,128)(2,1)S(1)} %get-tuple-element.29), channel_id=12, replica_groups=mesh['sp'=8,'tp'=4] {'sp'}, dimensions={2}, use_global_device_ids=true | all-gather | bytes 36864 | tf_op jit(solution)/shard_map/all_gather | solution.py:42
  429.7 0.3 fusion.19
  430.0 0.8 fusion.3
  430.9 21.2 %reduce-scatter.11.cloned.1.call-done = bf16[256,64]{0,1:T(8,128)(2,1)} async-done(((bf16[1024,64]{0,1:T(8,128)(2,1)}), bf16[256,64]{0,1:T(8,128)(2,1)}) %reduce-scatter.11.cloned.1.call-update) | async-done | bytes 32784 | tf_op jit(solution)/shard_map/reduce_scatter | solution.py:35
  (42 shorter events, 0.3 us)
Async XLA Ops:
  6.5 0.9 copy-start.2
  6.5 170.8 %reduce-scatter.5.cloned.1.call-start = ((), (), s32[]{:S(2)}) async-start(), calls=%async_computation.4 | async-start | bytes 163840 | tf_op jit(solution)/shard_map/reduce_scatter | solution.py:35
  7.4 6.8 %copy-start = (bf16[4,128,128]{2,1,0:T(8,128)(2,1)S(1)}, bf16[4,128,128]{2,1,0:T(8,128)(2,1)}, u32[]{:S(2)}) copy-start(bf16[4,128,128]{2,1,0:T(8,128)(2,1)} %param.8) | copy-start | bytes 393220
  46.0 6.2 %copy-start.1 = (bf16[4,128,128]{2,1,0:T(8,128)(2,1)S(1)}, bf16[4,128,128]{2,1,0:T(8,128)(2,1)}, u32[]{:S(2)}) copy-start(bf16[4,128,128]{2,1,0:T(8,128)(2,1)} %param.9) | copy-start | bytes 393220
  46.2 68.1 %collective-permute-start = (bf16[2,8,128]{2,1,0:T(8,128)(2,1)S(1)}, bf16[2,8,128]{2,1,0:T(8,128)(2,1)S(1)}, u32[]{:S(2)}, u32[]{:S(2)}) collective-permute-start(bf16[2,8,128]{2,1,0:T(8,128)(2,1)S(1)} %get-tuple-element.25), channel_id=1, source_target_pairs={{0,4},{4,8},{8,12},{12,16},{16,20},{20,24},{24,28},{1,5},{5,9},{9,... | collective-permute-start | bytes 12296 | tf_op jit(solution)/shard_map/ppermute | solution.py:24
  49.5 64.8 %collective-permute-start.1 = (bf16[2,8,128]{2,1,0:T(8,128)(2,1)S(1)}, bf16[2,8,128]{2,1,0:T(8,128)(2,1)S(1)}, u32[]{:S(2)}, u32[]{:S(2)}) collective-permute-start(bf16[2,8,128]{2,1,0:T(8,128)(2,1)S(1)} %get-tuple-element.26), channel_id=1, source_target_pairs={{4,0},{8,4},{12,8},{16,12},{20,16},{24,20},{28,24},{5,1},{9,5},{13... | collective-permute-start | bytes 12296 | tf_op jit(solution)/shard_map/ppermute | solution.py:26
  50.8 0.7 copy-start.3
  51.5 0.7 copy-start.4
  115.4 166.8 %reduce-scatter.7.cloned.1.call-start = ((), (), s32[]{:S(2)}) async-start(), calls=%async_computation.5 | async-start | bytes 163840 | tf_op jit(solution)/shard_map/reduce_scatter | solution.py:35
  183.4 35.9 %collective-permute-start.2 = (bf16[2,8,128]{2,1,0:T(8,128)(2,1)S(1)}, bf16[2,8,128]{2,1,0:T(8,128)(2,1)S(1)}, u32[]{:S(2)}, u32[]{:S(2)}) collective-permute-start(bf16[2,8,128]{2,1,0:T(8,128)(2,1)S(1)} %get-tuple-element.23), channel_id=1, source_target_pairs={{0,4},{4,8},{8,12},{12,16},{16,20},{20,24},{24,28},{1,5},{5,9},{9,... | collective-permute-start | bytes 12296 | tf_op jit(solution)/shard_map/ppermute | solution.py:24
  187.0 32.3 %collective-permute-start.3 = (bf16[2,8,128]{2,1,0:T(8,128)(2,1)S(1)}, bf16[2,8,128]{2,1,0:T(8,128)(2,1)S(1)}, u32[]{:S(2)}, u32[]{:S(2)}) collective-permute-start(bf16[2,8,128]{2,1,0:T(8,128)(2,1)S(1)} %get-tuple-element.24), channel_id=1, source_target_pairs={{4,0},{8,4},{12,8},{16,12},{20,16},{24,20},{28,24},{5,1},{9,5},{13... | collective-permute-start | bytes 12296 | tf_op jit(solution)/shard_map/ppermute | solution.py:26
  220.5 167.0 %reduce-scatter.9.cloned.1.call-start = ((), (), s32[]{:S(2)}) async-start(), calls=%async_computation.6 | async-start | bytes 163840 | tf_op jit(solution)/shard_map/reduce_scatter | solution.py:35
  288.3 36.2 %collective-permute-start.4 = (bf16[2,8,128]{2,1,0:T(8,128)(2,1)S(1)}, bf16[2,8,128]{2,1,0:T(8,128)(2,1)S(1)}, u32[]{:S(2)}, u32[]{:S(2)}) collective-permute-start(bf16[2,8,128]{2,1,0:T(8,128)(2,1)S(1)} %get-tuple-element.21), channel_id=1, source_target_pairs={{0,4},{4,8},{8,12},{12,16},{16,20},{20,24},{24,28},{1,5},{5,9},{9,... | collective-permute-start | bytes 12296 | tf_op jit(solution)/shard_map/ppermute | solution.py:24
  292.2 32.3 %collective-permute-start.5 = (bf16[2,8,128]{2,1,0:T(8,128)(2,1)S(1)}, bf16[2,8,128]{2,1,0:T(8,128)(2,1)S(1)}, u32[]{:S(2)}, u32[]{:S(2)}) collective-permute-start(bf16[2,8,128]{2,1,0:T(8,128)(2,1)S(1)} %get-tuple-element.22), channel_id=1, source_target_pairs={{4,0},{8,4},{12,8},{16,12},{20,16},{24,20},{28,24},{5,1},{9,5},{13... | collective-permute-start | bytes 12296 | tf_op jit(solution)/shard_map/ppermute | solution.py:26
  325.7 126.4 %reduce-scatter.11.cloned.1.call-start = ((), (), s32[]{:S(2)}) async-start(), calls=%async_computation.7 | async-start | bytes 163840 | tf_op jit(solution)/shard_map/reduce_scatter | solution.py:35
  393.5 36.2 %collective-permute-start.6 = (bf16[2,8,128]{2,1,0:T(8,128)(2,1)S(1)}, bf16[2,8,128]{2,1,0:T(8,128)(2,1)S(1)}, u32[]{:S(2)}, u32[]{:S(2)}) collective-permute-start(bf16[2,8,128]{2,1,0:T(8,128)(2,1)S(1)} %get-tuple-element.15), channel_id=1, source_target_pairs={{0,4},{4,8},{8,12},{12,16},{16,20},{20,24},{24,28},{1,5},{5,9},{9,... | collective-permute-start | bytes 12296 | tf_op jit(solution)/shard_map/ppermute | solution.py:24
  397.4 32.3 %collective-permute-start.7 = (bf16[2,8,128]{2,1,0:T(8,128)(2,1)S(1)}, bf16[2,8,128]{2,1,0:T(8,128)(2,1)S(1)}, u32[]{:S(2)}, u32[]{:S(2)}) collective-permute-start(bf16[2,8,128]{2,1,0:T(8,128)(2,1)S(1)} %get-tuple-element.16), channel_id=1, source_target_pairs={{4,0},{8,4},{12,8},{16,12},{20,16},{24,20},{28,24},{5,1},{9,5},{13... | collective-permute-start | bytes 12296 | tf_op jit(solution)/shard_map/ppermute | solution.py:26
Sparse Core Ops, SparseCore 0:
  115.6 20.8 reduce-scatter.4
  220.6 21.0 reduce-scatter.6
  325.8 21.0 reduce-scatter.8
  431.0 21.0 reduce-scatter.10
where the time goes:
time: 459 us
  blocking collectives  395 us (86%)
  waiting for transfers between devices  21.3 us (5%)
  starting transfers between devices  20 us (4%)
  between operations  13.4 us (3%)
  matrix products  5.24 us (1%)
    all_gather x4, blocking collectives, fetch_output(): lax.all_gather(out_weight[layer_index], 'sp', axis=1, tiled=True)  125 us
    all_gather x4, blocking collectives, taken_in(): lax.all_gather(part, axis, axis=dim, tiled=True)  124 us
    all_gather x4, blocking collectives, fetch_output(): lax.all_gather(mixing[layer_index], 'sp', axis=1, tiled=True)  123 us
    all_gather x4, blocking collectives, run_layer(): gathered = lax.all_gather(state_now, 'tp', axis=2, tiled=True)  23.5 us
    reduce_scatter x4, waiting for transfers between devices, scattered(): lax.psum_scatter(everything.astype(jnp.bfloat16), axis, scatter_dimension...  21.2 us
    ppermute x4, starting transfers between devices, extended_2(): lax.ppermute(tail, axis, [(i, (i + 1) % count) for i in range(ends)])  14.7 us
  transfers between devices with their start and end apart: 12, of which 1 were waited for; matrix products, arithmetic and copies ran while one was open for 0% of the time, Pallas kernels for 0%

commit v1 on v0

v1 whole, which is shorter than its diff:
```python
import functools

import jax
import jax.numpy as jnp
from jax import lax
from jax.experimental import pallas as pl
from jax.experimental.pallas import tpu as pltpu
from jax.sharding import PartitionSpec as P

F32, BF16 = jnp.float32, jnp.bfloat16
MINOR = 2


def kernel(sp_size, halo, act, gain, w_in, w_out, mix, scale, out, g_in, g_out, g_mix, st0, *rest):
    layers, in_rows, cols = w_in.shape
    seqs, toks, blk = act.shape
    width = gain.shape[1]
    major = sp_size // MINOR
    bufs = [rest[5 * l : 5 * l + 5] for l in range(layers)]
    (s_z, r_z, s_y, r_y, s_own, s_act, r_act, s_ar, r_ar) = rest[5 * layers :]
    sp, tp = lax.axis_index("sp"), lax.axis_index("tp")
    a, b = sp // MINOR, sp % MINOR
    q, h = tp // 2, tp % 2
    h0 = layers * halo

    def near(x):
        return lax.rem(x + sp_size, sp_size)

    def remote(src, dst, ss, rs, sp_to, tp_to):
        return pltpu.make_async_remote_copy(
            src_ref=src, dst_ref=dst, send_sem=ss, recv_sem=rs,
            device_id={"sp": sp_to, "tp": tp_to}, device_id_type=pl.DeviceIdType.MESH,
        )

    tp_peers = [lax.rem(tp + k, 4) for k in range(1, 4)]
    z_peers = [lax.rem(a + k, major) * MINOR + b for k in range(1, major)]
    y_peer = a * MINOR + (1 - b)

    barrier = pltpu.get_barrier_semaphore()
    everyone = [(sp, t) for t in tp_peers] + [(p, tp) for p in z_peers]
    everyone += [(y_peer, tp), (near(sp - 1), tp), (near(sp + 1), tp)]
    for s_to, t_to in everyone:
        pl.semaphore_signal(
            barrier, inc=1, device_id={"sp": s_to, "tp": t_to}, device_id_type=pl.DeviceIdType.MESH
        )
    owns = [(w_in, g_in), (w_out, g_out), (mix, g_mix)]
    own_copies = [
        pltpu.make_async_copy(src, dst.at[:, sp], s_own.at[i]) for i, (src, dst) in enumerate(owns)
    ]
    for c in own_copies:
        c.start()
    pl.semaphore_wait(barrier, len(everyone))

    pending = []

    def z_send(kind, l):
        src, dst = owns[kind]
        for k in range(1, major):
            c = remote(src.at[l], dst.at[l, sp], s_z.at[kind, l, k], r_z.at[kind, l, k], z_peers[k - 1], tp)
            c.start()
            pending.append(c)

    def y_send(kind, l, k):
        src, dst = owns[kind]
        origin = lax.rem(a - k + major, major) * MINOR + b
        block = src.at[l] if k == 0 else dst.at[l, origin]
        c = remote(block, dst.at[l, origin], s_y.at[kind, l, k], r_y.at[kind, l, k], y_peer, tp)
        c.start()
        pending.append(c)

    def forward(kind, l):
        src, dst = owns[kind]
        for k in range(1, major):
            origin = lax.rem(a - k + major, major) * MINOR + b
            remote(src.at[l], dst.at[l, origin], s_z.at[kind, l, k], r_z.at[kind, l, k], y_peer, tp).wait_recv()
            y_send(kind, l, k)

    def arrived(kind, l):
        src, dst = owns[kind]
        for k in range(major):
            origin = lax.rem(a - k + major, major) * MINOR + (1 - b)
            remote(src.at[l], dst.at[l, origin], s_y.at[kind, l, k], r_y.at[kind, l, k], y_peer, tp).wait_recv()

    def launch(kind, l):
        z_send(kind, l)
        y_send(kind, l, 0)

    has_left, has_right = sp > 0, sp < sp_size - 1
    left_rows, own_rows, right_rows = pl.ds(0, h0), pl.ds(h0, toks), pl.ds(h0 + toks, h0)
    to_right = remote(
        act.at[:, pl.ds(toks - h0, h0)], st0.at[h, q, :, left_rows], s_act.at[0, 0], r_act.at[0, 0], near(sp + 1), tp
    )
    to_left = remote(
        act.at[:, pl.ds(0, h0)], st0.at[h, q, :, right_rows], s_act.at[1, 0], r_act.at[1, 0], near(sp - 1), tp
    )
    pl.when(has_right)(to_right.start)
    pl.when(has_left)(to_left.start)
    launch(0, 0)
    own_out = []
    for k in range(1, 4):
        c = remote(act, st0.at[h, q, :, own_rows], s_act.at[2, k], r_act.at[2, k], sp, tp_peers[k - 1])
        c.start()
        own_out.append(c)
    launch(2, 0)
    launch(1, 0)
    st0[h, q, :, h0 : h0 + toks, :] = act[...]

    def spread(side, rows):
        return [
            remote(st0.at[h, q, :, rows], st0.at[h, q, :, rows], s_act.at[side, k], r_act.at[side, k], sp, tp_peers[k - 1])
            for k in range(1, 4)
        ]

    def take_side(side, rows, incoming):
        def yes():
            incoming.wait_recv()
            for c in spread(side, rows):
                c.start()

        return yes

    def blank(rows):
        def fill():
            st0[:, :, :, rows, :] = jnp.zeros((2, 2, seqs, h0, blk), BF16)

        return fill

    pl.when(has_left)(take_side(0, left_rows, to_right))
    pl.when(has_right)(take_side(1, right_rows, to_left))
    pl.when(jnp.logical_not(has_left))(blank(left_rows))
    pl.when(jnp.logical_not(has_right))(blank(right_rows))
    forward(0, 0)
    forward(2, 0)
    forward(1, 0)
    if layers > 1:
        launch(0, 1)
        launch(2, 1)
        launch(1, 1)
    for c in own_out:
        c.wait()

    def finish_side(side, rows):
        def yes():
            for c in spread(side, rows):
                c.wait()

        return yes

    pl.when(has_left)(finish_side(0, left_rows))
    pl.when(has_right)(finish_side(1, right_rows))
    for c in own_copies:
        c.wait()
    arrived(0, 0)

    seq_len = toks * sp_size
    half_window = lax.shift_left(jnp.int32(1), tp)

    def centring(l, n_in, n_out):
        base = sp * toks - (layers - l) * halo
        pos = base + halo + lax.broadcasted_iota(jnp.int32, (n_out, n_in), 0)
        src = base + lax.broadcasted_iota(jnp.int32, (n_out, n_in), 1)
        low = jnp.maximum(pos - half_window, 0)
        high = jnp.minimum(pos + half_window, seq_len)
        band = jnp.where((src >= low) & (src < high), 1.0, 0.0).astype(BF16)
        col = base + halo + lax.broadcasted_iota(jnp.int32, (n_out, 1), 0)
        count = jnp.minimum(col + half_window, seq_len) - jnp.maximum(col - half_window, 0)
        return band, 1.0 / jnp.maximum(count, 1).astype(F32)

    def state_of(l, s, hh, qq):
        return st0[hh, qq, s] if l == 0 else bufs[l - 1][4][s, hh, qq]

    def pooled_of(l, s):
        xs = [state_of(l, s, t % 2, t // 2).astype(F32) for t in range(4)]
        total = sum(jnp.sum(x * x, axis=-1, keepdims=True) for x in xs)
        inv = lax.rsqrt(total * (1.0 / width) + 1e-06)
        weight = g_in[l].reshape(width, cols)
        acc = None
        for t in range(4):
            normed = (xs[t] * inv * gain[l : l + 1, t * blk : (t + 1) * blk]).astype(BF16)
            term = jnp.dot(normed, weight[t * blk : (t + 1) * blk], preferred_element_type=F32)
            acc = term if acc is None else acc + term
        return acc.astype(BF16)

    def out_partial(l, s, pooled, band, inv_count):
        part = bufs[l][0]
        n_out = band.shape[0]
        sums = jnp.dot(band, pooled, preferred_element_type=F32)
        centred = (sums * inv_count - pooled.astype(F32)[halo : halo + n_out]).astype(BF16)
        mixing = g_mix[l].astype(F32).reshape(cols, cols).astype(BF16)
        mixed = jnp.dot(centred, mixing, preferred_element_type=F32)
        joined = (mixed * scale[l : l + 1, :]).astype(BF16)
        per = sp_size // 4
        for t in range(4):
            weight = jnp.concatenate([g_out[l, j] for j in range(t * per, (t + 1) * per)], axis=1)
            part[s, t % 2, t // 2] = jnp.dot(joined, weight, preferred_element_type=F32).astype(BF16)

    core_peer, far_peer = q * 2 + (1 - h), (1 - q) * 2 + h

    for l in range(layers):
        last = l == layers - 1
        n_in = toks + 2 * (layers - l) * halo
        n_out = n_in - 2 * halo
        part, r1, hf, r2, nxt = bufs[l]
        band, inv_count = centring(l, n_in, n_out)

        def stage(i, s, src, dst, peer):
            c = remote(src, dst, s_ar.at[i, l, s], r_ar.at[i, l, s], sp, peer)
            c.start()
            pending.append(c)
            return c

        first, second, third = [], [], []
        for s in range(seqs):
            if l > 0:
                gathers[s].wait_recv()
            pooled = pooled_of(l, s)
            if s == 0:
                arrived(2, l)
                arrived(1, l)
            out_partial(l, s, pooled, band, inv_count)
            first.append(stage(0, s, part.at[s, 1 - h], r1.at[s], core_peer))
        if not last:
            forward(0, l + 1)
        for s in range(seqs):
            first[s].wait_recv()
            hf[s] = (part[s, h].astype(F32) + r1[s].astype(F32)).astype(BF16)
            if last:
                second.append(stage(1, s, hf.at[s, 1 - q], r2.at[s, 0], far_peer))
            else:
                second.append(stage(1, s, hf.at[s], r2.at[s], far_peer))
        if not last:
            forward(2, l + 1)
            forward(1, l + 1)
        if l + 2 < layers:
            for kind in (0, 2, 1):
                launch(kind, l + 2)
        for s in range(seqs):
            second[s].wait_recv()
            if last:
                out[s] = (hf[s, q].astype(F32) + r2[s, 0].astype(F32)).astype(BF16)
            else:
                nxt[s, h] = (hf[s].astype(F32) + r2[s].astype(F32)).astype(BF16)
                third.append(stage(2, s, nxt.at[s, h], nxt.at[s, h], core_peer))
        gathers = third
        if not last:
            arrived(0, l + 1)

    pl.when(has_right)(to_right.wait_send)
    pl.when(has_left)(to_left.wait_send)
    for c in pending:
        c.wait_send()


def body(activations, norm_gain, in_weight, out_weight, mixing, pool_scale):
    sp_size, tp_size = lax.axis_size("sp"), lax.axis_size("tp")
    layers, in_rows, cols = in_weight.shape
    seqs, toks, blk = activations.shape
    groups = mixing.shape[1] * tp_size
    halo = 2 ** (groups - 1)
    assert tp_size == 4 and mixing.shape[1] == 1 and sp_size % 4 == 0 and layers * halo <= toks
    mixing = mixing.reshape(layers, mixing.shape[2], mixing.shape[3])
    major = sp_size // MINOR
    n0 = toks + 2 * layers * halo
    scratch = [
        pltpu.VMEM((layers, sp_size, in_rows, cols), BF16),
        pltpu.VMEM((layers, sp_size) + out_weight.shape[1:], BF16),
        pltpu.VMEM((layers, sp_size) + mixing.shape[1:], BF16),
        pltpu.VMEM((2, 2, seqs, n0, blk), BF16),
    ]
    for l in range(layers):
        n = n0 - 2 * (l + 1) * halo
        scratch += [
            pltpu.VMEM((seqs, 2, 2, n, blk), BF16),
            pltpu.VMEM((seqs, 2, n, blk), BF16),
            pltpu.VMEM((seqs, 2, n, blk), BF16),
            pltpu.VMEM((seqs, 2, n, blk), BF16),
            pltpu.VMEM((seqs, 2, 2, n, blk), BF16),
        ]
    dma = pltpu.SemaphoreType.DMA
    scratch += [
        dma((3, layers, major)), dma((3, layers, major)),
        dma((3, layers, major)), dma((3, layers, major)),
        dma((3,)), dma((3, 4)), dma((3, 4)), dma((3, layers, seqs)), dma((3, layers, seqs)),
    ]
    return pl.pallas_call(
        functools.partial(kernel, sp_size, halo),
        out_shape=jax.ShapeDtypeStruct(activations.shape, BF16),
        in_specs=[pl.BlockSpec(memory_space=pltpu.VMEM)] * 6,
        out_specs=pl.BlockSpec(memory_space=pltpu.VMEM),
        scratch_shapes=scratch,
        compiler_params=pltpu.CompilerParams(collective_id=0, has_side_effects=True),
    )(activations, norm_gain, in_weight, out_weight, mixing, pool_scale)


def solution(mesh):
    return jax.shard_map(
        body,
        mesh=mesh,
        in_specs=(
            P(None, "sp", "tp"),
            P(),
            P(None, "sp", "tp"),
            P(None, "tp", "sp"),
            P(None, "tp", "sp", None),
            P(None, "tp"),
        ),
        out_specs=P(None, "sp", "tp"),
        check_vma=False,
    )
```

time: 459 us -> 51.3 us (0.11)
  blocking collectives: 395 us -> 0 us
  Pallas kernels: 0 us -> 49.7 us
  waiting for transfers between devices: 21.3 us -> 0 us
  starting transfers between devices: 20 us -> 0 us
  between operations: 13.4 us -> 0.01 us
  matrix products: 5.24 us -> 0 us
    all_gather x16 -> x0, blocking collectives: 395 us -> none  [the longest x4 125 us: fetch_output(): lax.all_gather(out_weight[layer_index], 'sp', axis=1, tiled=True)]
    pallas_call x0 -> x1, Pallas kernels: none -> 49.7 us  [body(): pl.pallas_call(functools.partial(kernel, sp_size, halo), out_shape=jax.Sh...]
    reduce_scatter x4 -> x0, waiting for transfers between devices: 21.2 us -> none  [scattered(): lax.psum_scatter(everything.astype(jnp.bfloat16), axis, scatter_dimension...]
    ppermute x8 -> x0, starting transfers between devices: 19.9 us -> none  [the longest x4 14.7 us: extended_2(): lax.ppermute(tail, axis, [(i, (i + 1) % count) for i in range(ends)])]
    dot_general x12 -> x0, matrix products: 5.24 us -> none  [the longest x4 3.27 us: term_rows(): lax.dot_general(weight_cols, joined, (((0,), (1,)), ((), ())), preferred_...]
  transfers between devices with their start and end apart: 12 -> 0, of which waited for: 1 -> 0; matrix products, arithmetic and copies ran while one was open for 0% -> 0% of each run, Pallas kernels for 0% -> 0%
where the time goes in v1:
time: 51.3 us; the launch traced here: 51.1 us
  Pallas kernels  49.7 us (97%)
  local copies, waits for them, and re-layouts  1.38 us (3%)
    pallas_call x1, Pallas kernels, body(): pl.pallas_call(functools.partial(kernel, sp_size, halo), out_shape=jax.Sh...  49.7 us
    unnamed x1, local copies, waits for them, and re-layouts  1.38 us

profile of v1, /device:TPU:0, one launch (start us, length us, event | category | flops | bytes accessed | tf_op | source)
XLA Modules:
  0.0 51.1 jit_solution(11351295523068727506)
XLA Ops:
  0.0 49.7 %shard_map.64 = bf16[2,32,256]{2,1,0:T(8,128)(2,1)} custom-call(bf16[2,32,256]{2,1,0:T(8,128)(2,1)} %act.1, f32[4,1024]{1,0:T(4,128)} %gain.1, bf16[4,128,128]{2,1,0:T(8,128)(2,1)} %w_in.1, bf16[4,128,128]{2,1,0:T(8,128)(2,1)} %w_out.1, bf16[4,16,128]{2,1,0:T(8,128)(2,1)} %bitcast.1, f32[4,128]{1,0:T(4,128)} %scale.1), custom_call_target="tpu_custom_call" | custom-call | tf_op jit(solution)/shard_map/pallas_call | solution.py:285
  49.7 1.4 %copy.8 = bf16[2,32,256]{2,1,0:T(8,128)(2,1)} copy(bf16[2,32,256]{2,1,0:T(8,128)(2,1)} %shard_map.64) | data formatting | bytes 65536

commit v2 on v1

--- a/solution.py
+++ b/solution.py
@@ -11,7 +11,7 @@
 MINOR = 2
 
 
-def kernel(sp_size, halo, act, gain, w_in, w_out, mix, scale, out, g_in, g_out, g_mix, st0, *rest):
+def kernel(sp_size, halo, act_in, gain_in, w_in, w_out, mix, scale_in, out, act, gain, scale, g_in, g_out, g_mix, st0, *rest):
     layers, in_rows, cols = w_in.shape
     seqs, toks, blk = act.shape
     width = gain.shape[1]
@@ -36,6 +36,11 @@
     z_peers = [lax.rem(a + k, major) * MINOR + b for k in range(1, major)]
     y_peer = a * MINOR + (1 - b)
 
+    owns = [(w_in, g_in), (w_out, g_out), (mix, g_mix)]
+    placed = [(act_in, act), (w_in, g_in.at[:, sp]), (w_out, g_out.at[:, sp]), (mix, g_mix.at[:, sp])]
+    placed += [(gain_in, gain), (scale_in, scale)]
+    own_copies = [pltpu.make_async_copy(src, dst, s_own.at[i]) for i, (src, dst) in enumerate(placed)]
+
     barrier = pltpu.get_barrier_semaphore()
     everyone = [(sp, t) for t in tp_peers] + [(p, tp) for p in z_peers]
     everyone += [(y_peer, tp), (near(sp - 1), tp), (near(sp + 1), tp)]
@@ -43,12 +48,10 @@
         pl.semaphore_signal(
             barrier, inc=1, device_id={"sp": s_to, "tp": t_to}, device_id_type=pl.DeviceIdType.MESH
         )
-    owns = [(w_in, g_in), (w_out, g_out), (mix, g_mix)]
-    own_copies = [
-        pltpu.make_async_copy(src, dst.at[:, sp], s_own.at[i]) for i, (src, dst) in enumerate(owns)
-    ]
     for c in own_copies:
         c.start()
+    for c in own_copies:
+        c.wait()
     pl.semaphore_wait(barrier, len(everyone))
 
     pending = []
@@ -56,34 +59,31 @@
     def z_send(kind, l):
         src, dst = owns[kind]
         for k in range(1, major):
-            c = remote(src.at[l], dst.at[l, sp], s_z.at[kind, l, k], r_z.at[kind, l, k], z_peers[k - 1], tp)
+            c = remote(dst.at[l, sp], dst.at[l, sp], s_z.at[kind, l, k], r_z.at[kind, l, k], z_peers[k - 1], tp)
             c.start()
             pending.append(c)
 
     def y_send(kind, l, k):
         src, dst = owns[kind]
         origin = lax.rem(a - k + major, major) * MINOR + b
-        block = src.at[l] if k == 0 else dst.at[l, origin]
-        c = remote(block, dst.at[l, origin], s_y.at[kind, l, k], r_y.at[kind, l, k], y_peer, tp)
+        c = remote(dst.at[l, origin], dst.at[l, origin], s_y.at[kind, l, k], r_y.at[kind, l, k], y_peer, tp)
         c.start()
         pending.append(c)
 
     def forward(kind, l):
         src, dst = owns[kind]
+        if (kind, l) != (0, 0):
+            y_send(kind, l, 0)
         for k in range(1, major):
             origin = lax.rem(a - k + major, major) * MINOR + b
-            remote(src.at[l], dst.at[l, origin], s_z.at[kind, l, k], r_z.at[kind, l, k], y_peer, tp).wait_recv()
+            remote(dst.at[l, origin], dst.at[l, origin], s_z.at[kind, l, k], r_z.at[kind, l, k], y_peer, tp).wait_recv()
             y_send(kind, l, k)
 
     def arrived(kind, l):
         src, dst = owns[kind]
         for k in range(major):
             origin = lax.rem(a - k + major, major) * MINOR + (1 - b)
-            remote(src.at[l], dst.at[l, origin], s_y.at[kind, l, k], r_y.at[kind, l, k], y_peer, tp).wait_recv()
-
-    def launch(kind, l):
-        z_send(kind, l)
-        y_send(kind, l, 0)
+            remote(dst.at[l, origin], dst.at[l, origin], s_y.at[kind, l, k], r_y.at[kind, l, k], y_peer, tp).wait_recv()
 
     has_left, has_right = sp > 0, sp < sp_size - 1
     left_rows, own_rows, right_rows = pl.ds(0, h0), pl.ds(h0, toks), pl.ds(h0 + toks, h0)
@@ -95,14 +95,15 @@
     )
     pl.when(has_right)(to_right.start)
     pl.when(has_left)(to_left.start)
-    launch(0, 0)
+    z_send(0, 0)
+    y_send(0, 0, 0)
     own_out = []
     for k in range(1, 4):
         c = remote(act, st0.at[h, q, :, own_rows], s_act.at[2, k], r_act.at[2, k], sp, tp_peers[k - 1])
         c.start()
         own_out.append(c)
-    launch(2, 0)
-    launch(1, 0)
+    z_send(2, 0)
+    z_send(1, 0)
     st0[h, q, :, h0 : h0 + toks, :] = act[...]
 
     def spread(side, rows):
@@ -132,10 +133,9 @@
     forward(0, 0)
     forward(2, 0)
     forward(1, 0)
-    if layers > 1:
-        launch(0, 1)
-        launch(2, 1)
-        launch(1, 1)
+    for l in range(1, layers):
+        for kind in (0, 2, 1):
+            z_send(kind, l)
     for c in own_out:
         c.wait()
 
@@ -148,8 +148,6 @@
 
     pl.when(has_left)(finish_side(0, left_rows))
     pl.when(has_right)(finish_side(1, right_rows))
-    for c in own_copies:
-        c.wait()
     arrived(0, 0)
 
     seq_len = toks * sp_size
@@ -231,9 +229,6 @@
         if not last:
             forward(2, l + 1)
             forward(1, l + 1)
-        if l + 2 < layers:
-            for kind in (0, 2, 1):
-                launch(kind, l + 2)
         for s in range(seqs):
             second[s].wait_recv()
             if last:
@@ -262,6 +257,9 @@
     major = sp_size // MINOR
     n0 = toks + 2 * layers * halo
     scratch = [
+        pltpu.VMEM(activations.shape, BF16),
+        pltpu.VMEM(norm_gain.shape, F32),
+        pltpu.VMEM(pool_scale.shape, F32),
         pltpu.VMEM((layers, sp_size, in_rows, cols), BF16),
         pltpu.VMEM((layers, sp_size) + out_weight.shape[1:], BF16),
         pltpu.VMEM((layers, sp_size) + mixing.shape[1:], BF16),
@@ -280,12 +278,12 @@
     scratch += [
         dma((3, layers, major)), dma((3, layers, major)),
         dma((3, layers, major)), dma((3, layers, major)),
-        dma((3,)), dma((3, 4)), dma((3, 4)), dma((3, layers, seqs)), dma((3, layers, seqs)),
+        dma((6,)), dma((3, 4)), dma((3, 4)), dma((3, layers, seqs)), dma((3, layers, seqs)),
     ]
     return pl.pallas_call(
         functools.partial(kernel, sp_size, halo),
         out_shape=jax.ShapeDtypeStruct(activations.shape, BF16),
-        in_specs=[pl.BlockSpec(memory_space=pltpu.VMEM)] * 6,
+        in_specs=[pl.BlockSpec(memory_space=pl.ANY)] * 6,
         out_specs=pl.BlockSpec(memory_space=pltpu.VMEM),
         scratch_shapes=scratch,
         compiler_params=pltpu.CompilerParams(collective_id=0, has_side_effects=True),

time: 51.3 us -> 54 us (1.053)
  Pallas kernels: 49.7 us -> 52.2 us
    pallas_call x1, Pallas kernels: 49.7 us -> 52.2 us  [body(): pl.pallas_call(functools.partial(kernel, sp_size, halo), out_shape=jax.Sh...]
where the time goes in v2:
time: 54 us; the launch traced here: 53.6 us
  Pallas kernels  52.2 us (97%)
  local copies, waits for them, and re-layouts  1.38 us (3%)
    pallas_call x1, Pallas kernels, body(): pl.pallas_call(functools.partial(kernel, sp_size, halo), out_shape=jax.Sh...  52.2 us
    unnamed x1, local copies, waits for them, and re-layouts  1.38 us

profile of v2, /device:TPU:0, one launch (start us, length us, event | category | flops | bytes accessed | tf_op | source)
XLA Modules:
  0.0 53.6 jit_solution(16854363425923828670)
XLA Ops:
  0.0 52.2 %shard_map.64 = bf16[2,32,256]{2,1,0:T(8,128)(2,1)} custom-call(bf16[2,32,256]{2,1,0:T(8,128)(2,1)} %act_in.1, f32[4,1024]{1,0:T(4,128)} %gain_in.1, bf16[4,128,128]{2,1,0:T(8,128)(2,1)} %w_in.1, bf16[4,128,128]{2,1,0:T(8,128)(2,1)} %w_out.1, bf16[4,16,128]{2,1,0:T(8,128)(2,1)} %bitcast.1, f32[4,128]{1,0:T(4,128)} %scale_in.1), custom_call_target="tpu_custom_call" | custom-call | tf_op jit(solution)/shard_map/pallas_call | solution.py:283
  52.2 1.4 %copy.8 = bf16[2,32,256]{2,1,0:T(8,128)(2,1)} copy(bf16[2,32,256]{2,1,0:T(8,128)(2,1)} %shard_map.64) | data formatting | bytes 65536

commit v3 on v2

--- a/solution.py
+++ b/solution.py
@@ -72,8 +72,6 @@
 
     def forward(kind, l):
         src, dst = owns[kind]
-        if (kind, l) != (0, 0):
-            y_send(kind, l, 0)
         for k in range(1, major):
             origin = lax.rem(a - k + major, major) * MINOR + b
             remote(dst.at[l, origin], dst.at[l, origin], s_z.at[kind, l, k], r_z.at[kind, l, k], y_peer, tp).wait_recv()
@@ -84,6 +82,10 @@
         for k in range(major):
             origin = lax.rem(a - k + major, major) * MINOR + (1 - b)
             remote(dst.at[l, origin], dst.at[l, origin], s_y.at[kind, l, k], r_y.at[kind, l, k], y_peer, tp).wait_recv()
+
+    def launch(kind, l):
+        z_send(kind, l)
+        y_send(kind, l, 0)
 
     has_left, has_right = sp > 0, sp < sp_size - 1
     left_rows, own_rows, right_rows = pl.ds(0, h0), pl.ds(h0, toks), pl.ds(h0 + toks, h0)
@@ -95,15 +97,14 @@
     )
     pl.when(has_right)(to_right.start)
     pl.when(has_left)(to_left.start)
-    z_send(0, 0)
-    y_send(0, 0, 0)
+    launch(0, 0)
     own_out = []
     for k in range(1, 4):
         c = remote(act, st0.at[h, q, :, own_rows], s_act.at[2, k], r_act.at[2, k], sp, tp_peers[k - 1])
         c.start()
         own_out.append(c)
-    z_send(2, 0)
-    z_send(1, 0)
+    launch(2, 0)
+    launch(1, 0)
     st0[h, q, :, h0 : h0 + toks, :] = act[...]
 
     def spread(side, rows):
@@ -133,9 +134,10 @@
     forward(0, 0)
     forward(2, 0)
     forward(1, 0)
-    for l in range(1, layers):
-        for kind in (0, 2, 1):
-            z_send(kind, l)
+    if layers > 1:
+        launch(0, 1)
+        launch(2, 1)
+        launch(1, 1)
     for c in own_out:
         c.wait()
 
@@ -229,6 +231,9 @@
         if not last:
             forward(2, l + 1)
             forward(1, l + 1)
+        if l + 2 < layers:
+            for kind in (0, 2, 1):
+                launch(kind, l + 2)
         for s in range(seqs):
             second[s].wait_recv()
             if last:

time: 54 us -> 51.5 us (0.954)
  Pallas kernels: 52.2 us -> 50 us
    pallas_call x1, Pallas kernels: 52.2 us -> 50 us  [body(): pl.pallas_call(functools.partial(kernel, sp_size, halo), out_shape=jax.Sh...]
where the time goes in v3:
time: 51.5 us; the launch traced here: 51.3 us
  Pallas kernels  50 us (97%)
  local copies, waits for them, and re-layouts  1.38 us (3%)
    pallas_call x1, Pallas kernels, body(): pl.pallas_call(functools.partial(kernel, sp_size, halo), out_shape=jax.Sh...  50 us
    unnamed x1, local copies, waits for them, and re-layouts  1.38 us

profile of v3, /device:TPU:0, one launch (start us, length us, event | category | flops | bytes accessed | tf_op | source)
XLA Modules:
  0.0 51.3 jit_solution(10055723101489760317)
XLA Ops:
  0.0 50.0 %shard_map.64 = bf16[2,32,256]{2,1,0:T(8,128)(2,1)} custom-call(bf16[2,32,256]{2,1,0:T(8,128)(2,1)} %act_in.1, f32[4,1024]{1,0:T(4,128)} %gain_in.1, bf16[4,128,128]{2,1,0:T(8,128)(2,1)} %w_in.1, bf16[4,128,128]{2,1,0:T(8,128)(2,1)} %w_out.1, bf16[4,16,128]{2,1,0:T(8,128)(2,1)} %bitcast.1, f32[4,128]{1,0:T(4,128)} %scale_in.1), custom_call_target="tpu_custom_call" | custom-call | tf_op jit(solution)/shard_map/pallas_call | solution.py:288
  50.0 1.4 %copy.8 = bf16[2,32,256]{2,1,0:T(8,128)(2,1)} copy(bf16[2,32,256]{2,1,0:T(8,128)(2,1)} %shard_map.64) | data formatting | bytes 65536
